TPU v7x, 512 devices: a whole 4x4x16 slice. The times are simulated.
512 devices in a mesh: sp: 16 (over z), fs: 4 (over y), tp: 8 (over x, core).
Axes of the slice: x: 4, y: 4, z: 16, core: 2. Of those that a mesh axis runs over, the one named last changes fastest.
Arguments:
- tokens: bfloat16 [8, 2048, 1024], P('tp', 'sp'), may hold values from -6 to 6
- in_gain: float32 [1024], replicated, may hold values from 0.1 to 1.9
- query_weight: bfloat16 [1024, 1024], P('sp', 'fs'), may hold values from -0.1875 to 0.1875
- key_weight: bfloat16 [1024, 256], P('sp', 'fs'), may hold values from -0.1875 to 0.1875
- value_weight: bfloat16 [1024, 256], P('sp', 'fs'), may hold values from -0.1875 to 0.1875
- attn_gate_weight: bfloat16 [1024, 1024], P('sp', 'fs'), may hold values from -0.1875 to 0.1875
- state_in_weight: bfloat16 [1024, 512], P('sp', 'fs'), may hold values from -0.1875 to 0.1875
- state_gate_weight: bfloat16 [1024, 512], P('sp', 'fs'), may hold values from -0.1875 to 0.1875
- sink_logits: float32 [16], P('fs'), may hold values from 2 to 6
- decay_rate: float32 [32, 64], P('fs'), may hold values from 0.05 to 1.5
- rotation: float32 [32, 64], P('fs'), may hold values from 0.3 to 1.5
- step_size: float32 [32], P('fs'), may hold values from 0.5 to 2
- input_real: float32 [32, 64, 16], P('fs'), may hold values from -1 to 1
- input_imag: float32 [32, 64, 16], P('fs'), may hold values from -1 to 1
- output_real: float32 [32, 16, 64], P('fs'), may hold values from -0.01171875 to 0.01171875
- output_imag: float32 [32, 16, 64], P('fs'), may hold values from -0.01171875 to 0.01171875
- skip_scale: float32 [512], P('fs'), may hold values from -4 to 4
- focus_result_coefficients: bfloat16 [1024, 1024], P('fs', 'sp'), may hold values from -1 to 1
- state_out_weight: bfloat16 [512, 1024], P('fs', 'sp'), may hold values from -0.25 to 0.25
- out_gain: float32 [1024], P('fs'), may hold values from 0.1 to 1.9
Outputs:
- layer_output: bfloat16 [8, 2048, 1024], P('tp', 'sp', 'fs')
All inputs are finite; a program needn't handle non-finite values.
Results may differ from a plain program's by a relative error of at most 0.015.
Values may be sent and summed in bfloat16 or wider, within the bound.
A program may use at most 64 MiB of HBM per device.

v0:
```python
import jax
import jax.numpy as jnp
from jax import lax
from jax.sharding import PartitionSpec as P

HEAD_DIM = 64
WINDOW = 128
GROUP = 16


epsilon = 1e-05
theta_base = 10000.0


def shortened(value):
    return jax.tree.map(lambda a: a.astype(jnp.bfloat16) if a.dtype == jnp.float32 else a, value)


def passed_along(value, axis, steps):
    count = lax.axis_size(axis)
    initial, last = max(0, -steps), min(count, count - steps)
    return lax.ppermute(value, axis, [(source, source + steps) for source in range(initial, last)])


def folded(shard, axis, dim, absorb, state):
    everything = jax.tree.map(lambda a: lax.all_gather(a, axis, axis=dim, tiled=True), shard)
    return absorb(state, everything, jnp.int32(0))


def prefix(value, axis, join, neutral, backward):
    count, mine = lax.axis_size(axis), lax.axis_index(axis)
    pieces = jax.tree.map(lambda part: lax.all_gather(part, axis), value)
    if backward:
        pieces = jax.tree.map(lambda part: part[::-1], pieces)
        mine = count - 1 - mine
    running = jax.tree.map(
        lambda part, zero: jnp.full_like(part, 0) + jnp.asarray(zero, part.dtype), value, neutral
    )

    def hop(position, running):
        longer = join(running, jax.tree.map(lambda part: part[position], pieces))
        return jax.tree.map(lambda new, old: jnp.where(position < mine, new, old), longer, running)

    return lax.fori_loop(0, count - 1, hop, running)


def joined_along(pieces, dim):
    shape = list(pieces.shape[1:])
    shape[dim] *= pieces.shape[0]
    return jnp.moveaxis(pieces, 0, dim).reshape(shape)


def gather_packed(arrays, axis, dims):
    vector = jnp.concatenate([a.reshape(-1) for a in arrays])
    lines, at, gathered = lax.all_gather(vector, axis), 0, []
    for a, dim in zip(arrays, dims):
        pieces = lines[:, at : at + a.size].reshape(-1, *a.shape)
        gathered.append(joined_along(pieces, dim))
        at += a.size
    return tuple(gathered)


def scattered(product, rows, axis):
    everything = product(jnp.int32(0), lax.axis_size(axis) * rows)
    own = lax.psum_scatter(everything.astype(jnp.bfloat16), axis, scatter_dimension=0, tiled=True)
    return own.astype(jnp.float32)


def together(arrays, axis):
    ends = [0]
    for a in arrays:
        ends.append(ends[-1] + a.size)
    running = lax.psum(jnp.concatenate([a.ravel() for a in arrays]), axis)
    return tuple(running[b:e].reshape(a.shape) for a, b, e in zip(arrays, ends, ends[1:]))


def layer_norm(values, gain):
    center = jnp.mean(values, axis=-1, keepdims=True)
    spread = jnp.mean(jnp.square(values - center), axis=-1, keepdims=True)
    return (values - center) * lax.rsqrt(spread + epsilon) * gain


def rotate(values, positions):
    half = HEAD_DIM // 2
    inv_freq = jnp.power(theta_base, -jnp.arange(half, dtype=jnp.float32) / half)
    angles = positions.astype(jnp.float32)[:, None] * inv_freq
    cosine = jnp.cos(angles)[:, None, :]
    sine = jnp.sin(angles)[:, None, :]
    first = values[..., :half].astype(jnp.float32)
    second = values[..., half:].astype(jnp.float32)
    turned = jnp.concatenate(
        [first * cosine - second * sine, second * cosine + first * sine], axis=-1
    )
    return turned.astype(jnp.bfloat16)


def discretize(decay_rate, rotation, step_size, input_real, input_imag, sequence_extent):
    real_rate = -decay_rate / sequence_extent
    time_step = step_size[:, None]
    magnitude = jnp.exp(real_rate * time_step)
    decay_real = magnitude * jnp.cos(rotation * time_step)
    decay_imag = magnitude * jnp.sin(rotation * time_step)
    denominator = real_rate * real_rate + rotation * rotation
    factor_real = ((decay_real - 1.0) * real_rate + decay_imag * rotation) / denominator
    factor_imag = (decay_imag * real_rate - (decay_real - 1.0) * rotation) / denominator
    drive_real = factor_real[..., None] * input_real - factor_imag[..., None] * input_imag
    drive_imag = factor_real[..., None] * input_imag + factor_imag[..., None] * input_real
    return (decay_real, decay_imag, drive_real, drive_imag)


def combine_pair(earlier, later):
    first_real, leading_imaginary_part, first_state_real, first_state_imag = earlier
    second_real, second_imag, second_state_real, second_state_imag = later
    return (
        second_real * first_real - second_imag * leading_imaginary_part,
        second_real * leading_imaginary_part + second_imag * first_real,
        second_real * first_state_real - second_imag * first_state_imag + second_state_real,
        second_real * first_state_imag + second_imag * first_state_real + second_state_imag,
    )


def window_attention(queries, key_rows, value_rows, sink_logits, offset):
    sequence_extent = queries.shape[0]
    hop_count = (WINDOW + sequence_extent - 2) // sequence_extent
    stacked = jnp.stack([key_rows, value_rows])
    blocks = [stacked]
    carried = stacked
    for repeat in range(hop_count):
        carried = passed_along(shortened(carried), "sp", 1).astype(carried.dtype)
        blocks = [carried] + blocks
    joined = jnp.concatenate(blocks, axis=1)
    near_keys = joined[0]
    near_values = joined[1]
    kv_local = key_rows.shape[1]
    per_group = queries.shape[1] // kv_local
    grouped = queries.reshape(sequence_extent, kv_local, per_group, HEAD_DIM)
    scores = jnp.einsum(
        "qkrd,ckd->krqc", grouped, near_keys, preferred_element_type=jnp.float32
    ) * HEAD_DIM ** (-0.5)
    query_pos = offset + jnp.arange(sequence_extent, dtype=jnp.int32)
    key_pos = (
        offset
        - hop_count * sequence_extent
        + jnp.arange((hop_count + 1) * sequence_extent, dtype=jnp.int32)
    )
    differ = query_pos[:, None] - key_pos[None, :]
    allowed = (differ >= 0) & (differ < WINDOW) & (key_pos >= 0)[None, :]
    scores = jnp.where(allowed[None, None], scores, -jnp.inf)
    sink = sink_logits.reshape(kv_local, per_group)[:, :, None, None]
    largest = jnp.maximum(jnp.max(scores, axis=-1, keepdims=True), sink)
    weights = jnp.exp(scores - largest)
    weights = weights / (jnp.sum(weights, axis=-1, keepdims=True) + jnp.exp(sink - largest))
    attended = jnp.einsum(
        "krqc,ckd->qkrd",
        weights.astype(jnp.bfloat16),
        near_values,
        preferred_element_type=jnp.float32,
    )
    return attended.reshape(sequence_extent, -1)


def local(
    tokens,
    in_gain,
    query_weight,
    key_weight,
    value_weight,
    attn_gate_weight,
    state_in_weight,
    state_gate_weight,
    sink_logits,
    decay_rate,
    rotation,
    step_size,
    input_real,
    input_imag,
    output_real,
    output_imag,
    skip_scale,
    focus_result_coefficients,
    state_out_weight,
    out_gain,
):
    highest = lax.Precision.DEFAULT
    sequence_extent = tokens.shape[1]
    width = tokens.shape[2]
    offset = lax.axis_index("sp") * sequence_extent
    total_length = sequence_extent * lax.axis_size("sp")
    normed = layer_norm(tokens[0].astype(jnp.float32), in_gain).astype(jnp.bfloat16)
    incoming_coefficients = (
        query_weight,
        key_weight,
        value_weight,
        attn_gate_weight,
        state_in_weight,
        state_gate_weight,
    )
    blank_entries = tuple(
        (
            jnp.zeros((sequence_extent, number_grid.shape[1]), jnp.float32)
            for number_grid in incoming_coefficients
        )
    )

    def add_rows(totals, pieces, start):
        columns = lax.dynamic_slice_in_dim(normed, start, pieces[0].shape[0], 1)
        return tuple(
            (
                total + jnp.dot(columns, piece, preferred_element_type=jnp.float32)
                for total, piece in zip(totals, pieces)
            )
        )

    projected = folded(
        (
            incoming_coefficients[0],
            incoming_coefficients[1],
            incoming_coefficients[2],
            incoming_coefficients[3],
            incoming_coefficients[4],
            incoming_coefficients[5],
        ),
        "sp",
        0,
        add_rows,
        blank_entries,
    )
    queries_raw, keys_raw, values_raw, attn_gate, state_input, state_gate = [
        result.astype(jnp.bfloat16) for result in projected
    ]
    positions = offset + jnp.arange(sequence_extent, dtype=jnp.int32)
    queries = rotate(queries_raw.reshape(sequence_extent, -1, HEAD_DIM), positions)
    key_rows = rotate(keys_raw.reshape(sequence_extent, -1, HEAD_DIM), positions)
    value_rows = values_raw.reshape(sequence_extent, -1, HEAD_DIM)
    decay_real, decay_imag, drive_real, drive_imag = discretize(
        decay_rate, rotation, step_size, input_real, input_imag, total_length
    )
    group_count = decay_rate.shape[0]
    inputs_float = state_input.astype(jnp.float32).reshape(sequence_extent, group_count, GROUP)
    attended = window_attention(queries, key_rows, value_rows, sink_logits, offset)
    gated_attn = (jax.nn.sigmoid(attn_gate.astype(jnp.float32)) * attended).astype(jnp.bfloat16)
    push_real = jnp.einsum("sgh,gph->sgp", inputs_float, drive_real, precision=highest)
    push_imag = jnp.einsum("sgh,gph->sgp", inputs_float, drive_imag, precision=highest)
    powers_real = jnp.broadcast_to(decay_real, push_real.shape)
    powers_imag = jnp.broadcast_to(decay_imag, push_imag.shape)
    power_real, power_imag, state_real, state_imag = lax.associative_scan(
        combine_pair, (powers_real, powers_imag, push_real, push_imag), axis=0
    )
    ones = jnp.ones(decay_real.shape, jnp.float32)
    nothing_values = jnp.zeros(decay_real.shape, jnp.float32)
    entering = prefix(
        (power_real[-1], power_imag[-1], state_real[-1], state_imag[-1]),
        "sp",
        combine_pair,
        (ones, nothing_values, nothing_values, nothing_values),
        False,
    )
    carry_real = entering[2]
    carry_imag = entering[3]
    full_real = state_real + power_real * carry_real - power_imag * carry_imag
    full_imag = state_imag + power_real * carry_imag + power_imag * carry_real
    final_reading = jnp.einsum(
        "sgp,ghp->sgh", full_real, output_real, precision=highest
    ) - jnp.einsum("sgp,ghp->sgh", full_imag, output_imag, precision=highest)
    final_reading = final_reading + skip_scale.reshape(group_count, GROUP) * inputs_float
    final_reading = final_reading.reshape(sequence_extent, -1)
    gated_state = (
        jax.nn.gelu(final_reading, approximate=False)
        * jax.nn.sigmoid(state_gate.astype(jnp.float32))
    ).astype(jnp.bfloat16)
    attn_columns, state_columns = gather_packed(
        (focus_result_coefficients, state_out_weight), "sp", (1, 1)
    )
    feature_rows = width // lax.axis_size("fs")

    def term(start, count):
        part_attn = lax.dynamic_slice_in_dim(attn_columns, start, count, 1)
        part_state = lax.dynamic_slice_in_dim(state_columns, start, count, 1)
        first = lax.dot_general(
            part_attn, gated_attn, (((0,), (1,)), ((), ())), preferred_element_type=jnp.float32
        )
        second = lax.dot_general(
            part_state, gated_state, (((0,), (1,)), ((), ())), preferred_element_type=jnp.float32
        )
        return first + second

    mixed = scattered(term, feature_rows, "fs").T
    first_sum, second_sum = together(
        (jnp.sum(mixed, axis=-1), jnp.sum(mixed * mixed, axis=-1)), "fs"
    )
    center = first_sum / width
    centered = mixed - center[:, None]
    spread = second_sum / width - center * center
    result = centered * lax.rsqrt(spread[:, None] + epsilon) * out_gain
    return result.astype(jnp.bfloat16)[None]


def solution(mesh):
    return jax.shard_map(
        local,
        mesh=mesh,
        in_specs=(
            P("tp", "sp", None),
            P(),
            P("sp", "fs"),
            P("sp", "fs"),
            P("sp", "fs"),
            P("sp", "fs"),
            P("sp", "fs"),
            P("sp", "fs"),
            P("fs"),
            P("fs", None),
            P("fs", None),
            P("fs"),
            P("fs", None, None),
            P("fs", None, None),
            P("fs", None, None),
            P("fs", None, None),
            P("fs"),
            P("fs", "sp"),
            P("fs", "sp"),
            P("fs"),
        ),
        out_specs=P("tp", "sp", "fs"),
        check_vma=False,
    )
```

profile of v0, /device:TPU:6, one launch (start us, length us, event | category | flops | bytes accessed | tf_op | source)
XLA Modules:
  0.0 486.9 jit_solution(12778902601040429019)
XLA Ops:
  6.6 1.1 convert_reduce_fusion
  8.4 36.9 %all_gather.39 = bf16[1024,64]{1,0:T(8,128)(2,1)S(1)} all-gather(bf16[64,64]{1,0:T(8,128)(2,1)S(1)} %copy-done.25), channel_id=1, replica_groups=mesh['sp'=16,'fs'=4,'tp'=8] {'sp'}, dimensions={0}, use_global_device_ids=true | all-gather | bytes 139264 | tf_op jit(solution)/shard_map/all_gather | solution.py:26
  45.4 27.4 %all_gather.40 = bf16[1024,64]{1,0:T(8,128)(2,1)S(1)} all-gather(bf16[64,64]{1,0:T(8,128)(2,1)S(1)} %copy-done.26), channel_id=1, replica_groups=mesh['sp'=16,'fs'=4,'tp'=8] {'sp'}, dimensions={0}, use_global_device_ids=true | all-gather | bytes 139264 | tf_op jit(solution)/shard_map/all_gather | solution.py:26
  74.6 4.5 collective-permute-start
  79.1 27.3 %all_gather.42 = bf16[1024,128]{1,0:T(8,128)(2,1)S(1)} all-gather(bf16[64,128]{1,0:T(8,128)(2,1)S(1)} %copy-done.27), channel_id=1, replica_groups=mesh['sp'=16,'fs'=4,'tp'=8] {'sp'}, dimensions={0}, use_global_device_ids=true | all-gather | bytes 278528 | tf_op jit(solution)/shard_map/all_gather | solution.py:26
  115.6 0.7 add.582
  116.4 0.9 multiply_add_fusion.1
  117.2 0.7 add.580
  118.6 0.8 multiply_cosine_fusion
  122.3 30.6 %all_gather.46 = f32[16,8,64]{2,1,0:T(8,128)} all-gather(f32[1,8,64]{2,1,0:T(8,128)S(1)} %slice_add_fusion.42), channel_id=1, replica_groups=mesh['sp'=16,'fs'=4,'tp'=8] {'sp'}, dimensions={0}, use_global_device_ids=true | all-gather | bytes 34816 | tf_op jit(solution)/shard_map/all_gather | solution.py:32
  154.0 29.2 %all_gather.45 = f32[16,8,64]{2,1,0:T(8,128)} all-gather(f32[1,8,64]{2,1,0:T(8,128)S(1)} %slice_add_fusion.43), channel_id=1, replica_groups=mesh['sp'=16,'fs'=4,'tp'=8] {'sp'}, dimensions={0}, use_global_device_ids=true | all-gather | bytes 34816 | tf_op jit(solution)/shard_map/all_gather | solution.py:32
  184.8 29.9 %all_gather.44 = f32[16,8,64]{2,1,0:T(8,128)} all-gather(f32[1,8,64]{2,1,0:T(8,128)S(1)} %slice_add_fusion.44), channel_id=1, replica_groups=mesh['sp'=16,'fs'=4,'tp'=8] {'sp'}, dimensions={0}, use_global_device_ids=true | all-gather | bytes 34816 | tf_op jit(solution)/shard_map/all_gather | solution.py:32
  214.7 1.7 pad_maximum_fusion.1
  216.4 28.6 %pad.224 = f32[128,8,64]{2,1,0:T(8,128)} pad(f32[64,8,64]{2,1,0:T(8,128)} %pad_maximum_fusion.1, f32[]{:T(128)} %constant.50.clone.1), padding=0_1_1x0_0_0x0_0_0 | pad | bytes 393220 | tf_op jit(solution)/shard_map/pad | solution.py:246
  245.0 19.7 %pad.225 = f32[128,8,64]{2,1,0:T(8,128)} pad(f32[64,8,64]{2,1,0:T(8,128)S(1)} %copy-done.8, f32[]{:T(128)} %constant.50.clone.1), padding=1_0_1x0_0_0x0_0_0 | pad | bytes 393220 | tf_op jit(solution)/shard_map/pad | solution.py:246
  264.7 0.7 slice_add_fusion.45
  265.3 26.9 %all_gather.43 = f32[16,8,64]{2,1,0:T(8,128)S(1)} all-gather(f32[1,8,64]{2,1,0:T(8,128)S(1)} %slice_add_fusion.45), channel_id=1, replica_groups=mesh['sp'=16,'fs'=4,'tp'=8] {'sp'}, dimensions={0}, use_global_device_ids=true | all-gather | bytes 34816 | tf_op jit(solution)/shard_map/all_gather | solution.py:32
  292.3 10.5 %while.16 = (s32[]{:T(128)}, f32[8,64]{1,0:T(8,128)S(1)}, f32[8,64]{1,0:T(8,128)S(1)}, s32[]{:T(128)}, f32[16,8,64]{2,1,0:T(8,128)S(1)}, /*index=5*/f32[16,8,64]...) while((s32[]{:T(128)}, f32[8,64]{1,0:T(8,128)S(1)}, ...), condition=%wide.region_5.6_spmd.clone, body=%wide.region_4.5_spmd.clone.sunk | while | flops 6148 | bytes 16509 | solution.py:44
  292.3 0.7 fusion.217
  293.0 0.7 fusion.217
  293.7 0.7 fusion.217
  294.4 0.7 fusion.217
  295.1 0.7 fusion.217
  295.8 0.7 fusion.217
  296.5 0.7 fusion.217
  297.2 0.7 fusion.217
  297.9 0.7 fusion.217
  298.6 0.7 fusion.217
  299.3 0.7 fusion.217
  300.0 0.7 fusion.217
  300.7 0.7 fusion.217
  301.4 0.7 fusion.217
  302.1 0.7 fusion.217
  303.4 30.6 %all_gather.41 = bf16[1024,256]{1,0:T(8,128)(2,1)S(1)} all-gather(bf16[64,256]{1,0:T(8,128)(2,1)} %param.24), channel_id=1, replica_groups=mesh['sp'=16,'fs'=4,'tp'=8] {'sp'}, dimensions={0}, use_global_device_ids=true | all-gather | bytes 557056 | tf_op jit(solution)/shard_map/all_gather | solution.py:26
  334.1 0.9 convolution_convert_fusion
  335.0 1.6 copy.848
  337.7 31.0 %all-gather = bf16[393216]{0:T(1024)(128)(2,1)S(1)} all-gather(bf16[24576]{0:T(1024)(128)(2,1)S(1)} %pad_maximum_fusion.12), channel_id=2, replica_groups=mesh['sp'=16,'fs'=4,'tp'=8] {'sp'}, dimensions={0}, use_global_device_ids=true | all-gather | bytes 835584 | tf_op jit(solution)/shard_map/all_gather | solution.py:55
  368.7 32.3 %all_gather.38 = bf16[1024,256]{1,0:T(8,128)(2,1)} all-gather(bf16[64,256]{1,0:T(8,128)(2,1)S(1)} %copy-done.21), channel_id=1, replica_groups=mesh['sp'=16,'fs'=4,'tp'=8] {'sp'}, dimensions={0}, use_global_device_ids=true | all-gather | bytes 557056 | tf_op jit(solution)/shard_map/all_gather | solution.py:26
  401.0 1.3 multiply_add_fusion
  404.8 28.2 %all_gather.47 = bf16[1024,128]{1,0:T(8,128)(2,1)S(1)} all-gather(bf16[64,128]{1,0:T(8,128)(2,1)S(1)} %copy-done.29), channel_id=1, replica_groups=mesh['sp'=16,'fs'=4,'tp'=8] {'sp'}, dimensions={0}, use_global_device_ids=true | all-gather | bytes 278528 | tf_op jit(solution)/shard_map/all_gather | solution.py:26
  433.4 0.9 copy-done.1
  434.5 1.1 reshape.379
  437.8 0.8 maximum_maximum_fusion
  441.7 1.3 fusion.5
  443.0 26.0 %reduce-scatter.2.cloned.1.call-done = bf16[256,128]{1,0:T(8,128)(2,1)} async-done(((bf16[1024,128]{1,0:T(8,128)(2,1)}), bf16[256,128]{1,0:T(8,128)(2,1)}) %reduce-scatter.2.cloned.1.call-update) | async-done | bytes 65552 | tf_op jit(solution)/shard_map/reduce_scatter | solution.py:65
  469.0 1.0 convert_reduce_fusion.1
  470.0 8.5 %psum.7 = f32[256]{0:T(256)S(1)} all-reduce(f32[256]{0:T(256)S(1)} %pad_maximum_fusion.26), channel_id=1, replica_groups=mesh['sp'=16,'fs'=4,'tp'=8] {'fs'}, use_global_device_ids=true, to_apply=%region_9.10 | all-reduce | flops 256 | bytes 2048 | tf_op jit(solution)/shard_map/psum | solution.py:73
  479.3 0.7 copy.862
  (278 shorter events, 27.6 us)
Async XLA Ops:
  6.5 397.5 %copy-start = (f32[8,16,64]{2,1,0:T(8,128)S(1)}, f32[8,16,64]{2,1,0:T(8,128)}, u32[]{:S(2)}) copy-start(f32[8,16,64]{2,1,0:T(8,128)} %param.37) | copy-start | bytes 98308
  6.5 1.2 copy-start.5
  6.5 462.4 %reduce-scatter.2.cloned.1.call-start = ((), (), s32[]{:S(2)}) async-start(), calls=%async_computation.1 | async-start | bytes 327680 | tf_op jit(solution)/shard_map/reduce_scatter | solution.py:65
  6.6 66.9 %copy-start.32 = (f32[32]{0:T(128)}, f32[32]{0:T(128)S(1)}, u32[]{:S(2)}) copy-start(f32[32]{0:T(128)S(1)} %multiply_power_fusion) | copy-start | bytes 388
  7.7 98.7 %copy-start.40 = (f32[128]{0:T(128)}, f32[128]{0:T(128)S(1)}, u32[]{:S(2)}) copy-start(f32[128]{0:T(128)S(1)} %broadcast_multiply_fusion.2) | copy-start | bytes 1540
  7.7 0.7 copy-start.25
  7.9 98.5 %copy-start.49 = (f32[128]{0:T(128)}, f32[128]{0:T(128)S(1)}, u32[]{:S(2)}) copy-start(f32[128]{0:T(128)S(1)} %add_rsqrt_fusion.1) | copy-start | bytes 1540
  8.4 36.9 %copy-start.26 = (bf16[64,64]{1,0:T(8,128)(2,1)S(1)}, bf16[64,64]{1,0:T(8,128)(2,1)}, u32[]{:S(2)}) copy-start(bf16[64,64]{1,0:T(8,128)(2,1)} %param.26) | copy-start | bytes 24580
  45.4 28.1 %copy-start.34 = (f32[128]{0:T(128)}, f32[128]{0:T(128)S(1)}, u32[]{:S(2)}) copy-start(f32[128]{0:T(128)S(1)} %fusion.194) | copy-start | bytes 1540
  45.4 27.4 %copy-start.46 = (f32[1024]{0:T(1024)S(1)}, f32[1024]{0:T(1024)}, u32[]{:S(2)}) copy-start(f32[1024]{0:T(1024)} %param.23) | copy-start | bytes 12292
  74.0 5.1 %copy-start.39 = (f32[8]{0:T(128)S(1)}, f32[8]{0:T(128)}, u32[]{:S(2)}) copy-start(f32[8]{0:T(128)} %param.33) | copy-start | bytes 100
  74.0 5.1 %copy-start.27 = (bf16[64,128]{1,0:T(8,128)(2,1)S(1)}, bf16[64,128]{1,0:T(8,128)(2,1)}, u32[]{:S(2)}) copy-start(bf16[64,128]{1,0:T(8,128)(2,1)} %param.28) | copy-start | bytes 49156
  74.6 362.7 %collective-permute-start = (bf16[2,128,1,64]{1,3,2,0:T(8,128)(2,1)}, bf16[2,128,1,64]{1,3,2,0:T(8,128)(2,1)}, u32[]{:S(2)}, u32[]{:S(2)}) collective-permute-start(bf16[2,128,1,64]{1,3,2,0:T(8,128)(2,1)} %pad_maximum_fusion.13), channel_id=1, source_target_pairs={{0,32},{32,64},{64,96},{96,128},{128,160},{160,192},{192,224},{224... | collective-permute-start | bytes 98312 | tf_op jit(solution)/shard_map/ppermute | solution.py:22
  106.4 0.7 copy-start.30
  106.4 0.7 copy-start.31
  106.4 0.9 copy-start.15
  107.1 0.8 copy-start.14
  121.1 0.7 copy-start.22
  153.5 29.7 %copy-start.9 = (f32[64,8,64]{2,1,0:T(8,128)S(1)}, f32[64,8,64]{2,1,0:T(8,128)}, u32[]{:S(2)}) copy-start(f32[64,8,64]{2,1,0:T(8,128)} %add.582) | copy-start | bytes 393220
  183.3 0.9 copy-start.10
  184.7 60.2 %copy-start.2 = (f32[128,8,64]{2,1,0:T(8,128)}, f32[128,8,64]{2,1,0:T(8,128)S(1)}, u32[]{:S(2)}) copy-start(f32[128,8,64]{2,1,0:T(8,128)S(1)} %pad.226) | copy-start | bytes 786436
  216.4 28.6 %copy-start.8 = (f32[64,8,64]{2,1,0:T(8,128)S(1)}, f32[64,8,64]{2,1,0:T(8,128)}, u32[]{:S(2)}) copy-start(f32[64,8,64]{2,1,0:T(8,128)} %add.580) | copy-start | bytes 393220
  292.3 10.5 %copy-start.45 = (f32[128]{0:T(128)S(1)}, f32[128]{0:T(128)}, u32[]{:S(2)}) copy-start(f32[128]{0:T(128)} %param.38) | copy-start | bytes 1540
  303.4 30.6 %copy-start.6 = (bf16[1,128,1024]{2,1,0:T(8,128)(2,1)S(1)}, bf16[1,128,1024]{2,1,0:T(8,128)(2,1)}, u32[]{:S(2)}) copy-start(bf16[1,128,1024]{2,1,0:T(8,128)(2,1)} %param.22) | copy-start | bytes 786436
  303.4 30.6 %copy-start.41 = (f32[128]{0:T(128)S(1)}, f32[128]{0:T(128)}, u32[]{:S(2)}) copy-start(f32[128]{0:T(128)} %copy-done.40) | copy-start | bytes 1540
  303.4 30.6 %copy-start.47 = (f32[1024]{0:T(1024)S(1)}, f32[1024]{0:T(1024)}, u32[]{:S(2)}) copy-start(f32[1024]{0:T(1024)} %param.23) | copy-start | bytes 12292
  303.4 30.6 %copy-start.50 = (f32[128]{0:T(128)S(1)}, f32[128]{0:T(128)}, u32[]{:S(2)}) copy-start(f32[128]{0:T(128)} %copy-done.49) | copy-start | bytes 1540
  335.0 1.6 copy-start.20
  336.7 0.7 copy-start.28
  337.6 31.1 %copy-start.21 = (bf16[64,256]{1,0:T(8,128)(2,1)S(1)}, bf16[64,256]{1,0:T(8,128)(2,1)}, u32[]{:S(2)}) copy-start(bf16[64,256]{1,0:T(8,128)(2,1)} %param.27) | copy-start | bytes 98308
  337.6 63.4 %copy-start.3 = (f32[128,8,64]{2,1,0:T(8,128)S(1)}, f32[128,8,64]{2,1,0:T(8,128)}, u32[]{:S(2)}) copy-start(f32[128,8,64]{2,1,0:T(8,128)} %copy-done.2) | copy-start | bytes 786436
  337.7 63.4 %copy-start.4 = (f32[128,8,64]{2,1,0:T(8,128)S(1)}, f32[128,8,64]{2,1,0:T(8,128)}, u32[]{:S(2)}) copy-start(f32[128,8,64]{2,1,0:T(8,128)} %pad.224) | copy-start | bytes 786436
  401.0 1.4 copy-start.17
  402.4 0.8 copy-start.12
  402.4 0.8 copy-start.16
  403.2 0.7 copy-start.43
  403.2 0.7 copy-start.44
  403.2 0.8 copy-start.24
  404.1 0.7 copy-start.29
  433.3 0.9 copy-start.1
  435.6 1.0 slice-start
  437.1 0.7 copy-start.19
  439.8 1.0 copy-start.11
  439.8 1.0 copy-start.48
  440.0 1.0 copy-start.7
  440.1 0.9 copy-start.42
  440.1 0.9 copy-start.51
  469.0 9.5 %copy-start.13 = (bf16[256,128]{1,0:T(8,128)(2,1)S(1)}, bf16[256,128]{1,0:T(8,128)(2,1)}, u32[]{:S(2)}) copy-start(bf16[256,128]{1,0:T(8,128)(2,1)} %reduce-scatter.2.cloned.1.call-done) | copy-start | bytes 196612
  (7 other events, 4.5 us)
Sparse Core Ops, SparseCore 0:
  443.1 25.8 reduce-scatter.1
where the time goes:
time: 490 us; the launch traced here: 487 us
  blocking collectives  339 us (69%)
  local copies, waits for them, and re-layouts  72.9 us (15%)
  waiting for transfers between devices  26 us (5%)
  other arithmetic  24.5 us (5%)
  between operations  14.8 us (3%)
  matrix products  5.23 us (1%)
    all_gather x6, blocking collectives, folded(): lax.all_gather(a, axis, axis=dim, tiled=True)  183 us
    all_gather x4, blocking collectives, prefix(): pieces = jax.tree.map(lambda part: lax.all_gather(part, axis), value)  117 us
    pad x48, local copies, waits for them, and re-layouts, local(): lax.associative_scan(combine_pair, (powers_real, powers_imag, push_real,...  54.9 us
    all_gather x1, blocking collectives, gather_packed(): lines, at, gathered = (lax.all_gather(vector, axis), 0, [])  31 us
    reduce_scatter x1, waiting for transfers between devices, scattered(): lax.psum_scatter(everything.astype(jnp.bfloat16), axis, scatter_dimension...  26 us
    select_n x15, other arithmetic, hop(): jnp.where(position < mine, new, old)  10.5 us
  transfers between devices with their start and end apart: 2, of which 1 were waited for; matrix products, arithmetic and copies ran while one was open for 17% of the time, Pallas kernels for 0%

commit v1 on v0

v1 whole, which is shorter than its diff:
```python
import functools
import math

import jax
import jax.numpy as jnp
from jax import lax
from jax.experimental import pallas as pl
from jax.experimental.pallas import tpu as pltpu
from jax.sharding import PartitionSpec as P

HEAD_DIM = 64
GROUP = 16
STATE = 64
EPS = 1e-05
THETA = 10000.0
CHUNKS = 4

F32 = jnp.float32
BF16 = jnp.bfloat16
MESH = pl.DeviceIdType.MESH


def nn(a, b, precision=None):
    return lax.dot_general(
        a, b, (((1,), (0,)), ((), ())), precision=precision, preferred_element_type=F32
    )


def nt(a, b, precision=None):
    return lax.dot_general(
        a, b, (((1,), (1,)), ((), ())), precision=precision, preferred_element_type=F32
    )


def cmul(ar, ai, br, bi):
    return ar * br - ai * bi, ar * bi + ai * br


def kernel(
    sp_n, fs_n,
    tok, gain, wq, wk, wv, wg, wsi, wsg, sink, decay, rot, step, inr, ini, outr, outi,
    skip, wf, wso, ogain,
    out,
    W, normed, prow, Er, Ei, DM, CM, PW, cos_t, sin_t, Hr, Hi,
    kv_own, kv_prev, q_s, gate_s, sgate_s, u_s, att_s,
    s_own, s_in, mix_s, rs_out, rs_in, st_out, st_in,
    z_send, z_recv, c_send, c_recv, kv_send, kv_recv, s_send, s_recv,
    rs_send, rs_recv, st_send, st_recv,
):
    z = lax.axis_index("sp")
    y = lax.axis_index("fs")
    tp = lax.axis_index("tp")
    c = lax.rem(tp, 2)
    mate = tp + 1 - 2 * c
    up = lax.rem(z + 1, sp_n)
    down = lax.rem(z + sp_n - 1, sp_n)
    rows = wq.shape[0]
    tokens = tok.shape[1]
    piece = rows // CHUNKS
    n_up = sp_n // 2
    n_down = sp_n - 1 - n_up

    barrier = pltpu.get_barrier_semaphore()
    pl.semaphore_signal(barrier, inc=1, device_id={"sp": up}, device_id_type=MESH)
    pl.semaphore_signal(barrier, inc=1, device_id={"sp": down}, device_id_type=MESH)
    pl.semaphore_signal(barrier, inc=1, device_id={"tp": mate}, device_id_type=MESH)
    for d in range(1, fs_n):
        pl.semaphore_signal(
            barrier, inc=1, device_id={"fs": lax.rem(y + d, fs_n)}, device_id_type=MESH
        )

    own = pl.ds(pl.multiple_of(z * rows, rows), rows)
    W[0, own, 0:128] = wsi[...]
    W[0, own, 128:192] = wk[...]
    W[0, own, 192:256] = wv[...]
    W[0, own, 256:384] = wsg[...]
    W[0, own, 384:640] = wq[...]
    W[1, own, 0:256] = wg[...]
    eye = (
        lax.broadcasted_iota(jnp.int32, (rows, rows), 0)
        == lax.broadcasted_iota(jnp.int32, (rows, rows), 1)
    ).astype(BF16)
    W[1, own, 256:512] = nt(eye, wf[...]).astype(BF16)
    W[1, own, 512:640] = nt(eye, wso[...]).astype(BF16)

    pl.semaphore_wait(barrier, 3 + fs_n - 1)

    def shard(direction, k):
        return lax.rem(z + sp_n - k, sp_n) if direction == 0 else lax.rem(z + k, sp_n)

    def z_copy(direction, k, i):
        at = pl.multiple_of(shard(direction, k) * rows + i * piece, piece)
        ref = W.at[c, pl.ds(at, piece), :]
        return pltpu.make_async_remote_copy(
            src_ref=ref, dst_ref=ref,
            send_sem=z_send.at[direction], recv_sem=z_recv.at[direction, k, i],
            device_id={"sp": up if direction == 0 else down}, device_id_type=MESH,
        )

    def z_arrival(direction, k, i):
        at = pl.multiple_of(shard(direction, k + 1) * rows + i * piece, piece)
        ref = W.at[c, pl.ds(at, piece), :]
        return pltpu.make_async_remote_copy(
            src_ref=ref, dst_ref=ref,
            send_sem=z_send.at[direction], recv_sem=z_recv.at[direction, k, i],
            device_id={"sp": up if direction == 0 else down}, device_id_type=MESH,
        )

    def c_copy(direction, k):
        at = pl.multiple_of(shard(direction, k) * rows, rows)
        ref = W.at[c, pl.ds(at, rows), :]
        return pltpu.make_async_remote_copy(
            src_ref=ref, dst_ref=ref, send_sem=c_send, recv_sem=c_recv,
            device_id={"tp": mate}, device_id_type=MESH,
        )

    for i in range(CHUNKS):
        z_copy(0, 0, i).start()
        z_copy(1, 0, i).start()

    def work_norm(lo, hi):
        x = tok[0, lo:hi, :].astype(F32)
        width = x.shape[-1]
        center = jnp.sum(x, axis=-1, keepdims=True) / width
        x = x - center
        spread = jnp.sum(x * x, axis=-1, keepdims=True) / width
        normed[lo:hi, :] = (x * lax.rsqrt(spread + EPS) * gain[...]).astype(BF16)

    def work_rope():
        lane = lax.broadcasted_iota(jnp.int32, (1, 128), 1)
        inv = jnp.exp(lax.rem(lane, 32).astype(F32) * (-2.0 * math.log(THETA) / HEAD_DIM))
        r1, i1 = jnp.cos(inv), jnp.sin(inv)
        sub = lax.broadcasted_iota(jnp.int32, (8, 128), 0)
        br = jnp.ones((8, 128), F32)
        bi = jnp.zeros((8, 128), F32)
        pr, pi = jnp.ones((1, 128), F32), jnp.zeros((1, 128), F32)
        for r in range(1, 8):
            pr, pi = cmul(pr, pi, r1, i1)
            br = jnp.where(sub == r, pr, br)
            bi = jnp.where(sub == r, pi, bi)
        sr, si = cmul(pr, pi, r1, i1)
        full_r, full_i = br, bi
        while full_r.shape[0] < tokens:
            nr, ni = cmul(full_r, full_i, sr, si)
            full_r = jnp.concatenate([full_r, nr], axis=0)
            full_i = jnp.concatenate([full_i, ni], axis=0)
            sr, si = cmul(sr, si, sr, si)
        zr, zi = jnp.ones((1, 128), F32), jnp.zeros((1, 128), F32)
        bit = 1
        while bit < sp_n:
            on = jnp.full((1, 128), lax.rem(z // bit, 2), jnp.int32) == 1
            nr, ni = cmul(zr, zi, sr, si)
            zr = jnp.where(on, nr, zr)
            zi = jnp.where(on, ni, zi)
            sr, si = cmul(sr, si, sr, si)
            bit *= 2
        full_r, full_i = cmul(full_r, full_i, zr, zi)
        first = lax.rem(lax.broadcasted_iota(jnp.int32, (tokens, 128), 1), 64) < 32
        cos_t[...] = full_r
        sin_t[...] = jnp.where(first, -full_i, full_i)

    def work_rows():
        for g in range(8):
            at = slice(STATE * g, STATE * g + STATE)
            prow[0:1, at] = decay[g : g + 1, :]
            prow[1:2, at] = rot[g : g + 1, :]
            prow[2:3, at] = jnp.full((1, STATE), step[g], F32)

    def work_states():
        rate = -prow[0:1, :] / float(sp_n * tokens)
        turn = prow[1:2, :]
        dt = prow[2:3, :]
        size = jnp.exp(rate * dt)
        ar, ai = size * jnp.cos(turn * dt), size * jnp.sin(turn * dt)
        den = rate * rate + turn * turn
        prow[3:4, :] = ((ar - 1.0) * rate + ai * turn) / den
        prow[4:5, :] = (ai * rate - (ar - 1.0) * turn) / den
        sub = lax.broadcasted_iota(jnp.int32, (8, 512), 0)
        br = jnp.broadcast_to(ar, (8, 512))
        bi = jnp.broadcast_to(ai, (8, 512))
        pr, pi = ar, ai
        for r in range(1, 8):
            pr, pi = cmul(pr, pi, ar, ai)
            br = jnp.where(sub == r, pr, br)
            bi = jnp.where(sub == r, pi, bi)
        Er[0:8, :] = br
        Ei[0:8, :] = bi
        sr, si = pr, pi
        n = 8
        while n < tokens:
            nr, ni = cmul(Er[0:n, :], Ei[0:n, :], sr, si)
            Er[n : 2 * n, :] = nr
            Ei[n : 2 * n, :] = ni
            sr, si = cmul(sr, si, sr, si)
            n *= 2
        pr, pi = jnp.ones((1, 512), F32), jnp.zeros((1, 512), F32)
        for d in range(sp_n):
            PW[d, :, 0:512] = pr
            PW[d, :, 512:1024] = pi
            pr, pi = cmul(pr, pi, sr, si)

    def work_drive():
        pick = (
            lax.rem(lax.broadcasted_iota(jnp.int32, (128, GROUP), 0), GROUP)
            == lax.broadcasted_iota(jnp.int32, (128, GROUP), 1)
        ).astype(F32)
        high = lax.Precision.HIGHEST
        xr = nt(pick, inr[...].reshape(8 * STATE, GROUP), high)
        xi = nt(pick, ini[...].reshape(8 * STATE, GROUP), high)
        fr, fi = prow[3:4, :], prow[4:5, :]
        dr, di = cmul(fr, fi, xr, xi)
        same = (
            lax.broadcasted_iota(jnp.int32, (128, 512), 0) // GROUP
            == lax.broadcasted_iota(jnp.int32, (128, 512), 1) // STATE
        )
        DM[:, 0:512] = jnp.where(same, dr, 0.0).astype(BF16)
        DM[:, 512:1024] = jnp.where(same, di, 0.0).astype(BF16)

    def work_read():
        pick = (
            lax.rem(lax.broadcasted_iota(jnp.int32, (STATE, 512), 1), STATE)
            == lax.broadcasted_iota(jnp.int32, (STATE, 512), 0)
        ).astype(BF16)
        same = (
            lax.broadcasted_iota(jnp.int32, (128, 512), 0) // GROUP
            == lax.broadcasted_iota(jnp.int32, (128, 512), 1) // STATE
        )
        cr = nn(outr[...].reshape(128, STATE).astype(BF16), pick)
        ci = nn(outi[...].reshape(128, STATE).astype(BF16), pick)
        CM[:, 0:512] = jnp.where(same, cr, 0.0).astype(BF16)
        CM[:, 512:1024] = jnp.where(same, -ci, 0.0).astype(BF16)

    half = tokens // 2
    work = [
        functools.partial(work_norm, 0, half),
        functools.partial(work_norm, half, tokens),
        work_rope,
        work_rows,
        work_states,
        work_drive,
        work_read,
    ]
    for k in range(n_up):
        if k < len(work):
            work[k]()
        for i in range(CHUNKS):
            z_arrival(0, k, i).wait_recv()
            if k + 1 < n_up:
                z_copy(0, k + 1, i).start()
            if k < n_down:
                z_arrival(1, k, i).wait_recv()
                if k + 1 < n_down:
                    z_copy(1, k + 1, i).start()
        c_copy(0, k + 1).start()
        if k < n_down:
            c_copy(1, k + 1).start()
    others = pl.ds(0, (sp_n - 1) * rows)

    def c_total(h):
        ref = W.at[h, others, :]
        return pltpu.make_async_remote_copy(
            src_ref=ref, dst_ref=ref, send_sem=c_send, recv_sem=c_recv,
            device_id={"tp": mate}, device_id_type=MESH,
        )

    c_total(1 - c).wait_recv()

    lane128 = lax.broadcasted_iota(jnp.int32, (tokens, 128), 1)
    first = lax.rem(lane128, 64) < 32

    def turned(v, co, si):
        swapped = jnp.where(first, pltpu.roll(v, 96, 1), pltpu.roll(v, 32, 1))
        return v * co + swapped * si

    uk = nn(normed[...], W[0, :, 0:256])
    u = uk[:, 0:128].astype(BF16)
    kv = uk[:, 128:256].astype(BF16).astype(F32)
    key_part = lane128 < 64
    kv_own[...] = jnp.where(key_part, turned(kv, cos_t[...], sin_t[...]), kv).astype(BF16)
    u_s[...] = u
    kv_copy = pltpu.make_async_remote_copy(
        src_ref=kv_own, dst_ref=kv_prev, send_sem=kv_send, recv_sem=kv_recv,
        device_id={"sp": up}, device_id_type=MESH,
    )

    def shifted(v, n, sub):
        if n % 8 == 0:
            return jnp.concatenate([jnp.zeros((n, v.shape[1]), F32), v[: tokens - n, :]], axis=0)
        return jnp.where(sub >= n, pltpu.roll(v, n, 0), 0.0)

    sub128 = lax.broadcasted_iota(jnp.int32, (tokens, 128), 0)
    for b in range(4):
        at = slice(128 * b, 128 * b + 128)
        hr = nn(u, DM[:, at])
        hi = nn(u, DM[:, slice(512 + 128 * b, 640 + 128 * b)])
        n = 1
        while n < tokens:
            ar, ai = Er[n - 1 : n, at], Ei[n - 1 : n, at]
            mr, mi = cmul(ar, ai, shifted(hr, n, sub128), shifted(hi, n, sub128))
            hr, hi = hr + mr, hi + mi
            n *= 2
        Hr[:, at] = hr
        Hi[:, at] = hi
        s_own[:, at] = hr[tokens - 1 : tokens, :]
        s_own[:, slice(512 + 128 * b, 640 + 128 * b)] = hi[tokens - 1 : tokens, :]
    kv_copy.start()

    def s_copy(d):
        return pltpu.make_async_remote_copy(
            src_ref=s_own, dst_ref=s_in.at[d], send_sem=s_send.at[d], recv_sem=s_recv.at[d],
            device_id={"sp": lax.rem(z + d, sp_n)}, device_id_type=MESH,
        )

    qg = nn(normed[...], W[0, :, 256:640])
    for d in range(1, sp_n):
        @pl.when(z + d < sp_n)
        def _(d=d):
            s_copy(d).start()
    sgate_s[...] = jax.nn.sigmoid(qg[:, 0:128].astype(BF16).astype(F32))
    for b in range(2):
        raw = qg[:, 128 + 128 * b : 256 + 128 * b].astype(BF16).astype(F32)
        q_s[:, 128 * b : 128 * b + 128] = turned(raw, cos_t[...], sin_t[...]).astype(BF16)
    gate_s[...] = jax.nn.sigmoid(nn(normed[...], W[1, :, 0:256]).astype(BF16).astype(F32))

    kv_copy.wait_recv()
    mine = kv_own[...].astype(F32)
    past = kv_prev[...].astype(F32)
    low = lane128 < 64
    zero = jnp.zeros_like(mine)

    def sides(v):
        turned_v = pltpu.roll(v, 64, 1)
        keys = [jnp.where(low, v, zero).astype(BF16), jnp.where(low, zero, turned_v).astype(BF16)]
        vals = [jnp.where(low, turned_v, zero).astype(BF16), jnp.where(low, zero, v).astype(BF16)]
        return keys, vals

    mine_k, mine_v = sides(mine)
    past_k, past_v = sides(past)
    lower = lax.broadcasted_iota(jnp.int32, (tokens, tokens), 1) <= lax.broadcasted_iota(
        jnp.int32, (tokens, tokens), 0
    )
    has_past = jnp.full((tokens, tokens), z, jnp.int32) > 0
    for b in range(2):
        qb = q_s[:, 128 * b : 128 * b + 128]
        total = None
        for s in range(2):
            sc = jnp.where(lower, nt(qb, mine_k[s]), nt(qb, past_k[s])) * (HEAD_DIM ** -0.5)
            sc = jnp.where(lower | has_past, sc, -1e30)
            logit = sink[2 * b + s]
            top = jnp.maximum(jnp.max(sc, axis=-1, keepdims=True), logit)
            w = jnp.exp(sc - top)
            w = w / (jnp.sum(w, axis=-1, keepdims=True) + jnp.exp(logit - top))
            wz = jnp.zeros_like(w)
            part = nn(jnp.where(lower, w, wz).astype(BF16), mine_v[s])
            part = part + nn(jnp.where(lower, wz, w).astype(BF16), past_v[s])
            total = part if total is None else total + part
        at = slice(128 * b, 128 * b + 128)
        att_s[:, at] = (gate_s[:, at] * total).astype(BF16)

    mix_s[...] = nt(att_s[...], W[1, :, 256:512])

    cr = jnp.zeros((1, 512), F32)
    ci = jnp.zeros((1, 512), F32)
    for d in range(1, sp_n):
        @pl.when(z >= d)
        def _(d=d):
            s_copy(d).wait_recv()
        on = jnp.full((1, 512), z, jnp.int32) >= d
        tr, ti = cmul(
            PW[d - 1, :, 0:512], PW[d - 1, :, 512:1024], s_in[d, :, 0:512], s_in[d, :, 512:1024]
        )
        cr = cr + jnp.where(on, tr, 0.0)
        ci = ci + jnp.where(on, ti, 0.0)
    fr, fi = cmul(Er[...], Ei[...], cr, ci)
    reading = nt((Hr[...] + fr).astype(BF16), CM[:, 0:512])
    reading = reading + nt((Hi[...] + fi).astype(BF16), CM[:, 512:1024])
    reading = reading + skip[...] * u_s[...].astype(F32)
    gelu = 0.5 * reading * (1.0 + lax.erf(reading * math.sqrt(0.5)))
    gated_state = (gelu * sgate_s[...]).astype(BF16)

    width = mix_s.shape[1]
    feats = width // fs_n

    def rs_copy(d):
        return pltpu.make_async_remote_copy(
            src_ref=rs_out.at[d], dst_ref=rs_in.at[d],
            send_sem=rs_send.at[d], recv_sem=rs_recv.at[d],
            device_id={"fs": lax.rem(y + d, fs_n)}, device_id_type=MESH,
        )

    def features(d):
        at = pl.ds(pl.multiple_of(lax.rem(y + d, fs_n) * feats, feats), feats)
        return mix_s[:, at] + nt(gated_state, W[1, at, 512:640])

    order = [fs_n // 2] + [d for d in range(1, fs_n) if d != fs_n // 2]
    for d in order:
        rs_out[d] = features(d).astype(BF16)
    for d in order:
        rs_copy(d).start()
    mixed = features(0)
    for d in order[1:] + order[:1]:
        rs_copy(d).wait_recv()
        mixed = mixed + rs_in[d].astype(F32)

    mean = jnp.sum(mixed, axis=-1, keepdims=True) / feats
    dev = mixed - mean
    sq = jnp.sum(dev * dev, axis=-1, keepdims=True)
    tile = jnp.where(lane128 == 0, mean, jnp.where(lane128 == 1, sq, 0.0))
    st_out[...] = jnp.transpose(tile)[0:8, :]

    def st_copy(d):
        return pltpu.make_async_remote_copy(
            src_ref=st_out, dst_ref=st_in.at[d],
            send_sem=st_send.at[d], recv_sem=st_recv.at[d],
            device_id={"fs": lax.rem(y + d, fs_n)}, device_id_type=MESH,
        )

    for d in order:
        st_copy(d).start()
    tiles = [st_out[...]]
    for d in order[1:] + order[:1]:
        st_copy(d).wait_recv()
        tiles.append(st_in[d])
    mean_row = sum(t[0:1, :] for t in tiles) / fs_n
    sq_row = sum(t[1:2, :] + feats * jnp.square(t[0:1, :] - mean_row) for t in tiles)
    scale_row = lax.rsqrt(sq_row / width + EPS)
    sub_sq = lax.broadcasted_iota(jnp.int32, (128, 128), 0)
    both = jnp.where(sub_sq == 0, mean_row, jnp.where(sub_sq == 1, scale_row, 0.0))
    both = jnp.transpose(both)
    out[0] = ((mixed - both[:, 0:1]) * both[:, 1:2] * ogain[...]).astype(BF16)

    for direction, steps in ((0, n_up), (1, n_down)):
        ref = W.at[0, pl.ds(0, steps * rows), :]
        pltpu.make_async_remote_copy(
            src_ref=ref, dst_ref=ref,
            send_sem=z_send.at[direction], recv_sem=z_recv.at[direction, 0, 0],
            device_id={"sp": up}, device_id_type=MESH,
        ).wait_send()
    c_total(0).wait_send()
    kv_copy.wait_send()
    for d in range(1, sp_n):
        @pl.when(z + d < sp_n)
        def _(d=d):
            s_copy(d).wait_send()
    for d in order:
        rs_copy(d).wait_send()
        st_copy(d).wait_send()


def local(sp_n, fs_n, *args):
    (
        tokens, in_gain, query, key, value, attn_gate, state_in, state_gate, sink, decay, rotation,
        step, in_r, in_i, out_r, out_i, skip, focus, state_out, out_gain,
    ) = args
    t = tokens.shape[1]
    rows = query.shape[0]
    width = tokens.shape[2]
    feats = width // fs_n
    vm = pl.BlockSpec(memory_space=pltpu.VMEM)
    sm = pl.BlockSpec(memory_space=pltpu.SMEM)
    specs = [vm] * 8 + [sm, vm, vm, sm] + [vm] * 8
    n_up = sp_n // 2
    V, dma = pltpu.VMEM, pltpu.SemaphoreType.DMA
    return pl.pallas_call(
        functools.partial(kernel, sp_n, fs_n),
        out_shape=jax.ShapeDtypeStruct((1, t, feats), BF16),
        in_specs=specs,
        out_specs=vm,
        scratch_shapes=[
            V((2, sp_n * rows, 640), BF16), V((t, width), BF16), V((8, 512), F32),
            V((t, 512), F32), V((t, 512), F32), V((128, 1024), BF16), V((128, 1024), BF16),
            V((sp_n, 1, 1024), F32), V((t, 128), F32), V((t, 128), F32),
            V((t, 512), F32), V((t, 512), F32),
            V((t, 128), BF16), V((t, 128), BF16), V((t, 256), BF16), V((t, 256), F32),
            V((t, 128), F32), V((t, 128), BF16), V((t, 256), BF16),
            V((1, 1024), F32), V((sp_n, 1, 1024), F32), V((t, width), F32),
            V((fs_n, t, feats), BF16), V((fs_n, t, feats), BF16),
            V((8, 128), F32), V((fs_n, 8, 128), F32),
            dma((2,)), dma((2, n_up, CHUNKS)), dma, dma, dma, dma, dma((sp_n,)), dma((sp_n,)),
            dma((fs_n,)), dma((fs_n,)), dma((fs_n,)), dma((fs_n,)),
        ],
        compiler_params=pltpu.CompilerParams(
            collective_id=0, has_side_effects=True, vmem_limit_bytes=48 * 1024 * 1024
        ),
        name="layer",
    )(
        tokens, in_gain.reshape(1, -1), query, key, value, attn_gate, state_in, state_gate, sink,
        decay, rotation, step, in_r, in_i, out_r, out_i, skip.reshape(1, -1), focus, state_out,
        out_gain.reshape(1, -1),
    )


def solution(mesh):
    sizes = dict(mesh.shape)
    return jax.shard_map(
        functools.partial(local, sizes["sp"], sizes["fs"]),
        mesh=mesh,
        in_specs=(
            P("tp", "sp", None),
            P(),
            P("sp", "fs"),
            P("sp", "fs"),
            P("sp", "fs"),
            P("sp", "fs"),
            P("sp", "fs"),
            P("sp", "fs"),
            P("fs"),
            P("fs", None),
            P("fs", None),
            P("fs"),
            P("fs", None, None),
            P("fs", None, None),
            P("fs", None, None),
            P("fs", None, None),
            P("fs"),
            P("fs", "sp"),
            P("fs", "sp"),
            P("fs"),
        ),
        out_specs=P("tp", "sp", "fs"),
        check_vma=False,
    )
```

time: 490 us -> 60.5 us (0.12)
  blocking collectives: 339 us -> 0 us
  local copies, waits for them, and re-layouts: 72.9 us -> 3.24 us
  Pallas kernels: 0 us -> 56.5 us
  waiting for transfers between devices: 26 us -> 0 us
  other arithmetic: 24.5 us -> 0 us
  between operations: 14.8 us -> 0.24 us
  matrix products: 5.23 us -> 0 us
    all_gather x11 -> x0, blocking collectives: 330 us -> none  [the longest x6 183 us: folded(): lax.all_gather(a, axis, axis=dim, tiled=True)]
    pallas_call x0 -> x1, Pallas kernels: none -> 56.5 us  [local(): pl.pallas_call(functools.partial(kernel, sp_n, fs_n), out_shape=jax.Shape...]
    pad x48 -> x0, local copies, waits for them, and re-layouts: 54.9 us -> none  [local(): lax.associative_scan(combine_pair, (powers_real, powers_imag, push_real,...]
    reduce_scatter x1 -> x0, waiting for transfers between devices: 26 us -> none  [scattered(): lax.psum_scatter(everything.astype(jnp.bfloat16), axis, scatter_dimension...]
    select_n x15 -> x0, other arithmetic: 10.5 us -> none  [hop(): jnp.where(position < mine, new, old)]
    psum x1 -> x0, blocking collectives: 8.54 us -> none  [together(): running = lax.psum(jnp.concatenate([a.ravel() for a in arrays]), axis)]
    unnamed x106 -> x43, local copies, waits for them, and re-layouts: 9.68 us -> 3.24 us
    add x51 -> x0, other arithmetic: 6.41 us -> none  [the longest x27 2.43 us: local(): lax.associative_scan(combine_pair, (powers_real, powers_imag, push_real,...]
  transfers between devices with their start and end apart: 2 -> 0, of which waited for: 1 -> 0; matrix products, arithmetic and copies ran while one was open for 17% -> 0% of each run, Pallas kernels for 0% -> 0%
where the time goes in v1:
time: 60.5 us; the launch traced here: 59.9 us
  Pallas kernels  56.5 us (93%)
  local copies, waits for them, and re-layouts  3.24 us (5%)
    pallas_call x1, Pallas kernels, local(): pl.pallas_call(functools.partial(kernel, sp_n, fs_n), out_shape=jax.Shape...  56.5 us
    unnamed x43, local copies, waits for them, and re-layouts  3.24 us

profile of v1, /device:TPU:6, one launch (start us, length us, event | category | flops | bytes accessed | tf_op | source)
XLA Modules:
  0.0 59.9 jit_solution(6855791133313146402)
XLA Ops:
  0.0 0.0 copy-start.18
  0.0 0.0 copy-start.16
  0.0 0.9 %copy.24.wso = bf16[128,64]{1,0:T(8,128)(2,1)S(1)} copy(bf16[128,64]{0,1:T(8,128)(2,1)} %param.38) | data formatting | bytes 32768 | tf_op args[18]
  0.9 0.0 copy-done.18
  0.9 0.1 copy.23.wf
  1.0 0.0 copy-done.16
  1.0 0.0 copy-start.17
  1.0 0.0 copy-start
  1.0 0.1 copy.21.inr
  1.2 0.7 %copy-done.17 = f32[8,64,16]{1,2,0:T(8,128)S(1)} copy-done((f32[8,64,16]{1,2,0:T(8,128)S(1)}, f32[8,64,16]{1,2,0:T(8,128)}, u32[]{:S(2)}) %copy-start.17) | copy-done | bytes 32792
  1.8 0.0 copy-start.1
  1.8 0.0 copy-start.2
  1.9 0.0 copy-start.3
  1.9 0.0 copy-start.4
  1.9 0.0 copy-start.5
  1.9 0.0 copy-start.6
  1.9 0.0 copy-start.7
  1.9 0.0 copy-start.8
  1.9 0.0 copy-start.9
  1.9 0.0 copy-start.10
  1.9 0.0 copy-start.11
  1.9 0.0 copy-start.12
  2.0 0.0 copy-start.13
  2.0 0.0 copy-start.14
  2.0 0.0 copy-start.15
  2.0 0.1 copy.22.ini
  2.1 0.0 copy-done
  2.1 0.6 copy-done.1
  2.7 0.0 copy-done.2
  2.7 0.0 copy-done.3
  2.7 0.0 copy-done.4
  2.7 0.0 copy-done.5
  2.7 0.0 copy-done.6
  2.7 0.0 copy-done.7
  2.8 0.0 copy-done.8
  2.8 0.0 copy-done.9
  2.8 0.0 copy-done.10
  2.8 0.0 copy-done.11
  2.8 0.0 copy-done.12
  2.8 0.0 copy-done.13
  2.8 0.0 copy-done.14
  2.8 0.0 copy-done.15
  2.8 56.5 %layer.1 = bf16[1,128,256]{2,1,0:T(8,128)(2,1)S(1)} custom-call(bf16[1,128,1024]{2,1,0:T(8,128)(2,1)S(1)} %copy-done, f32[1,1024]{1,0:T(1,128)S(1)} %bitcast.3, bf16[64,256]{1,0:T(8,128)(2,1)S(1)} %copy-done.3, bf16[64,64]{1,0:T(8,128)(2,1)S(1)} %copy-done.5, bf16[64,64]{1,0:T(8,128)(2,1)S(1)} %copy-done.6, bf16[64,256]{1,0:T(8,128)(2,1)S(1)} %copy-done.4, ...), custom_call_target="tpu_custom_call" | custom-call | tf_op jit(solution)/shard_map/layer/pallas_call | solution.py:464
  59.3 0.6 %copy.26 = bf16[1,128,256]{2,1,0:T(8,128)(2,1)} copy(bf16[1,128,256]{2,1,0:T(8,128)(2,1)S(1)} %layer.1) | data formatting | bytes 131072
Async XLA Ops:
  0.0 0.9 %copy-start.18 = (bf16[256,64]{0,1:T(8,128)(2,1)S(1)}, bf16[256,64]{0,1:T(8,128)(2,1)}, u32[]{:S(2)}) copy-start(bf16[256,64]{0,1:T(8,128)(2,1)} %param.37) | copy-start | bytes 98308
  0.0 1.0 %copy-start.16 = (f32[8,64,16]{1,2,0:T(8,128)S(1)}, f32[8,64,16]{1,2,0:T(8,128)}, u32[]{:S(2)}) copy-start(f32[8,64,16]{1,2,0:T(8,128)} %param.32) | copy-start | bytes 98308
  1.0 0.8 %copy-start.17 = (f32[8,64,16]{1,2,0:T(8,128)S(1)}, f32[8,64,16]{1,2,0:T(8,128)}, u32[]{:S(2)}) copy-start(f32[8,64,16]{1,2,0:T(8,128)} %param.33) | copy-start | bytes 98308
  1.0 1.1 %copy-start = (bf16[1,128,1024]{2,1,0:T(8,128)(2,1)S(1)}, bf16[1,128,1024]{2,1,0:T(8,128)(2,1)}, u32[]{:S(2)}) copy-start(bf16[1,128,1024]{2,1,0:T(8,128)(2,1)} %tok.1) | copy-start | bytes 786436
  1.8 0.9 %copy-start.1 = (f32[8,16,64]{2,1,0:T(8,128)S(1)}, f32[8,16,64]{2,1,0:T(8,128)}, u32[]{:S(2)}) copy-start(f32[8,16,64]{2,1,0:T(8,128)} %outr.1) | copy-start | bytes 98308
  1.8 0.9 %copy-start.2 = (f32[8,16,64]{2,1,0:T(8,128)S(1)}, f32[8,16,64]{2,1,0:T(8,128)}, u32[]{:S(2)}) copy-start(f32[8,16,64]{2,1,0:T(8,128)} %outi.1) | copy-start | bytes 98308
  1.9 0.9 %copy-start.3 = (bf16[64,256]{1,0:T(8,128)(2,1)S(1)}, bf16[64,256]{1,0:T(8,128)(2,1)}, u32[]{:S(2)}) copy-start(bf16[64,256]{1,0:T(8,128)(2,1)} %wq.1) | copy-start | bytes 98308
  1.9 0.9 %copy-start.4 = (bf16[64,256]{1,0:T(8,128)(2,1)S(1)}, bf16[64,256]{1,0:T(8,128)(2,1)}, u32[]{:S(2)}) copy-start(bf16[64,256]{1,0:T(8,128)(2,1)} %wg.1) | copy-start | bytes 98308
  1.9 0.9 %copy-start.5 = (bf16[64,64]{1,0:T(8,128)(2,1)S(1)}, bf16[64,64]{1,0:T(8,128)(2,1)}, u32[]{:S(2)}) copy-start(bf16[64,64]{1,0:T(8,128)(2,1)} %wk.1) | copy-start | bytes 24580
  1.9 0.9 %copy-start.6 = (bf16[64,64]{1,0:T(8,128)(2,1)S(1)}, bf16[64,64]{1,0:T(8,128)(2,1)}, u32[]{:S(2)}) copy-start(bf16[64,64]{1,0:T(8,128)(2,1)} %wv.1) | copy-start | bytes 24580
  1.9 0.9 %copy-start.7 = (bf16[64,128]{1,0:T(8,128)(2,1)S(1)}, bf16[64,128]{1,0:T(8,128)(2,1)}, u32[]{:S(2)}) copy-start(bf16[64,128]{1,0:T(8,128)(2,1)} %wsi.1) | copy-start | bytes 49156
  1.9 0.9 %copy-start.8 = (bf16[64,128]{1,0:T(8,128)(2,1)S(1)}, bf16[64,128]{1,0:T(8,128)(2,1)}, u32[]{:S(2)}) copy-start(bf16[64,128]{1,0:T(8,128)(2,1)} %wsg.1) | copy-start | bytes 49156
  1.9 0.9 %copy-start.9 = (f32[1024]{0:T(1024)S(1)}, f32[1024]{0:T(1024)}, u32[]{:S(2)}) copy-start(f32[1024]{0:T(1024)} %param.21) | copy-start | bytes 12292
  1.9 0.9 %copy-start.10 = (f32[8,64]{1,0:T(8,128)S(1)}, f32[8,64]{1,0:T(8,128)}, u32[]{:S(2)}) copy-start(f32[8,64]{1,0:T(8,128)} %decay.1) | copy-start | bytes 6148
  1.9 0.9 %copy-start.11 = (f32[8,64]{1,0:T(8,128)S(1)}, f32[8,64]{1,0:T(8,128)}, u32[]{:S(2)}) copy-start(f32[8,64]{1,0:T(8,128)} %rot.1) | copy-start | bytes 6148
  1.9 0.9 %copy-start.12 = (f32[256]{0:T(256)S(1)}, f32[256]{0:T(256)}, u32[]{:S(2)}) copy-start(f32[256]{0:T(256)} %param.39) | copy-start | bytes 3076
  2.0 0.9 %copy-start.13 = (f32[4]{0:T(128)S(1)}, f32[4]{0:T(128)}, u32[]{:S(2)}) copy-start(f32[4]{0:T(128)} %sink.1) | copy-start | bytes 52
  2.0 0.9 %copy-start.14 = (f32[8]{0:T(128)S(1)}, f32[8]{0:T(128)}, u32[]{:S(2)}) copy-start(f32[8]{0:T(128)} %step.1) | copy-start | bytes 100
  2.0 0.9 %copy-start.15 = (f32[128]{0:T(128)S(1)}, f32[128]{0:T(128)}, u32[]{:S(2)}) copy-start(f32[128]{0:T(128)} %param.36) | copy-start | bytes 1540
